TPU v7x, 512 devices: a whole 4x8x8 slice. The times are simulated.
512 devices in a mesh: sp: 64 (over z, y), tp: 4 (over x), dp: 2 (over core).
Axes of the slice: x: 4, y: 8, z: 8, core: 2. Of those that a mesh axis runs over, the one named last changes fastest.
Arguments:
- latent: bfloat16 [2, 16384, 2048], P('dp', 'sp'), may hold values from -1.5 to 1.5
- condition: bfloat16 [2, 2048], P('dp', 'sp'), may hold values from -6 to 6
- context: bfloat16 [2, 1024, 2048], P('dp', 'sp'), may hold values from -6 to 6
- context_code: bfloat16 [2048], P('sp'), may hold values from -6 to 6
- shift_weight: bfloat16 [2048, 2048], P('sp', 'tp'), may hold values from -0.125 to 0.125
- scale_weight: bfloat16 [2048, 2048], P('sp', 'tp'), may hold values from -0.125 to 0.125
- gate_weight: bfloat16 [2048, 2048], P('sp', 'tp'), may hold values from -0.125 to 0.125
- norm_gain: float32 [2048], replicated, may hold values from 0.1 to 1.9
- query_weight: bfloat16 [2048, 1024], P(None, 'tp'), may hold values from -0.125 to 0.125
- key_weight: bfloat16 [2048, 256], P(None, 'tp'), may hold values from -0.125 to 0.125
- value_weight: bfloat16 [2048, 256], P(None, 'tp'), may hold values from -0.125 to 0.125
- output_weight: bfloat16 [1024, 2048], P('tp'), may hold values from -0.75 to 0.75
- query_gain: float32 [64], replicated, may hold values from 1 to 5.5
- key_gain: float32 [64], replicated, may hold values from 1 to 5.5
- context_bias: float32 [16], P('tp'), may hold values from 0.5 to 2
Outputs:
- updated: bfloat16 [2, 16384, 2048], P('dp', 'sp')
All inputs are finite; a program needn't handle non-finite values.
Results may differ from a plain program's by a relative error of at most 0.01405.
The roundings to bfloat16 on the way count: a program that leaves them out, or rounds other values in their place, can miss the bound.
Values may be sent and summed in bfloat16 or wider, within the bound.
A program may use at most 64 MiB of HBM per device.

v0:
```python
import math
import jax
import jax.numpy as jnp
from jax import lax
from jax.sharding import PartitionSpec as P

GRID_W = 64
norm_eps = 1e-06
rope_base = 10000.0


def from_everyone(array, axis):
    size = lax.axis_size(axis)
    return lax.all_to_all(
        jnp.broadcast_to(array[None], (size, *array.shape)), axis, 0, 0, tiled=True
    )


def of_everyone(array, axis):
    return from_everyone(array, axis).sum(axis=0)


def laid_out(pieces, dim):
    dims = list(pieces.shape[1:])
    dims[dim] *= pieces.shape[0]
    return jnp.moveaxis(pieces, 0, dim).reshape(dims)


def gathered_copies(array, axis, dim):
    pieces = from_everyone(array, axis)
    return laid_out(pieces, dim)


def cut_along(array, dim, size):
    before, after = (array.shape[:dim], array.shape[dim + 1 :])
    return jnp.moveaxis(array.reshape(*before, size, -1, *after), dim, 0)


def sent_and_summed(array, axis, dim):
    size = lax.axis_size(axis)
    pieces = lax.all_to_all(cut_along(array, dim, size), axis, 0, 0, tiled=True)
    return jnp.sum(pieces.astype(jnp.float32), axis=0)


def rotary_tables(position, grid_width, head_dim):
    grid_row = (position // grid_width).astype(jnp.float32)
    grid_col = (position % grid_width).astype(jnp.float32)
    quarter = head_dim // 4
    inverse = rope_base ** (-jnp.arange(quarter, dtype=jnp.float32) / quarter)
    angles = jnp.concatenate([grid_row[:, None] * inverse, grid_col[:, None] * inverse], axis=-1)
    return (jnp.cos(angles), jnp.sin(angles))


def head_norm(values, gain_row):
    return (
        values * lax.rsqrt(jnp.mean(values * values, axis=-1, keepdims=True) + norm_eps) * gain_row
    )


def rotate(values, cosine, sine_part):
    half_dim = values.shape[-1] // 2
    first_half = values[..., :half_dim]
    second_half = values[..., half_dim:]
    cos_rows = cosine[:, None, :]
    sin_rows = sine_part[:, None, :]
    return jnp.concatenate(
        [
            first_half * cos_rows - second_half * sin_rows,
            second_half * cos_rows + first_half * sin_rows,
        ],
        axis=-1,
    )


def modulated(tokens, gain_row, shift_row, scale_row):
    floats = tokens.astype(jnp.float32)
    normal = floats * lax.rsqrt(jnp.mean(floats * floats, axis=-1, keepdims=True) + norm_eps)
    return (normal * gain_row * (1.0 + scale_row) + shift_row).astype(jnp.bfloat16)


def on_device(
    latent,
    condition,
    context,
    context_code,
    shift_weight,
    scale_weight,
    gate_weight,
    norm_gain,
    query_weight,
    key_weight,
    value_weight,
    output_weight,
    query_gain,
    key_gain,
    context_bias,
):
    head_dim = query_gain.shape[0]
    tp_size = lax.axis_size("tp")
    activated = jax.nn.silu(condition[0].astype(jnp.float32)).astype(jnp.bfloat16)
    context_act = jax.nn.silu(context_code.astype(jnp.float32)).astype(jnp.bfloat16)
    partial_mod = jnp.stack(
        [
            jnp.dot(activated, shift_weight, preferred_element_type=jnp.float32),
            jnp.dot(activated, scale_weight, preferred_element_type=jnp.float32),
            jnp.dot(activated, gate_weight, preferred_element_type=jnp.float32),
            jnp.dot(context_act, shift_weight, preferred_element_type=jnp.float32),
            jnp.dot(context_act, scale_weight, preferred_element_type=jnp.float32),
        ]
    )
    summed = of_everyone(partial_mod, "sp")
    vectors = gathered_copies(summed, "tp", 1)
    normed = modulated(latent[0], norm_gain, vectors[0], vectors[1])
    query_cols = query_weight.shape[1]
    key_cols = key_weight.shape[1]
    projected = jnp.concatenate(
        [
            jnp.dot(normed, query_weight, preferred_element_type=jnp.float32),
            jnp.dot(normed, key_weight, preferred_element_type=jnp.float32),
            jnp.dot(normed, value_weight, preferred_element_type=jnp.float32),
        ],
        axis=1,
    )
    seq_rows = projected.shape[0]
    position = lax.axis_index("sp") * seq_rows + jnp.arange(seq_rows, dtype=jnp.int32)
    cosine, sine_part = rotary_tables(position, GRID_W, head_dim)
    group_size = query_cols // head_dim
    queries = projected[:, :query_cols].reshape(seq_rows, group_size, head_dim)
    queries = rotate(head_norm(queries, query_gain), cosine, sine_part).astype(jnp.bfloat16)
    latent_keys = projected[:, query_cols : query_cols + key_cols].reshape(seq_rows, 1, head_dim)
    latent_keys = rotate(head_norm(latent_keys, key_gain), cosine, sine_part).astype(jnp.bfloat16)
    latent_values = projected[:, query_cols + key_cols :].astype(jnp.bfloat16)
    key_value = jnp.concatenate([latent_keys.reshape(seq_rows, head_dim), latent_values], axis=1)
    context_normed = modulated(context[0], norm_gain, vectors[3], vectors[4])
    context_keys = head_norm(
        jnp.dot(context_normed, key_weight, preferred_element_type=jnp.float32), key_gain
    )
    context_values = jnp.dot(context_normed, value_weight, preferred_element_type=jnp.float32)
    context_kv = gathered_copies(
        jnp.concatenate(
            [context_keys.astype(jnp.bfloat16), context_values.astype(jnp.bfloat16)], axis=1
        ),
        "sp",
        0,
    )
    score_scale = head_dim ** (-0.5)
    query_rows = queries.transpose(1, 0, 2).reshape(group_size * seq_rows, head_dim)
    bias_rows = jnp.repeat(context_bias, seq_rows)
    context_scores = jnp.dot(
        query_rows, context_kv[:, :head_dim].T, preferred_element_type=jnp.float32
    )
    context_scores = context_scores * score_scale + bias_rows[:, None]
    first_max = context_scores.max(axis=1)
    context_exp = jnp.exp(context_scores - first_max[:, None])
    start_state = (
        first_max,
        context_exp.sum(axis=1),
        jnp.dot(
            context_exp.astype(jnp.bfloat16),
            context_kv[:, head_dim:],
            preferred_element_type=jnp.float32,
        ),
    )
    arrived = lax.all_gather(key_value, "sp", axis=0, tiled=True)
    arrived_rows = arrived.shape[0]
    block_rows = math.gcd(arrived_rows, 1024)
    blocks = arrived.reshape(arrived_rows // block_rows, block_rows, 2 * head_dim)

    def absorb_block(state_now, pair_block):
        old_max, old_total, old_accum = state_now
        scores = (
            jnp.dot(query_rows, pair_block[:, :head_dim].T, preferred_element_type=jnp.float32)
            * score_scale
        )
        new_max = jnp.maximum(old_max, scores.max(axis=1))
        factor = jnp.exp(old_max - new_max)
        weights = jnp.exp(scores - new_max[:, None])
        new_accum = old_accum * factor[:, None] + jnp.dot(
            weights.astype(jnp.bfloat16),
            pair_block[:, head_dim:],
            preferred_element_type=jnp.float32,
        )
        return ((new_max, old_total * factor + weights.sum(axis=1), new_accum), None)

    final_state, unused = lax.scan(absorb_block, start_state, blocks)
    row_max, totals, accum = final_state
    attended = (accum / totals[:, None]).astype(jnp.bfloat16)
    attended = (
        attended.reshape(group_size, seq_rows, head_dim)
        .transpose(1, 0, 2)
        .reshape(seq_rows, query_cols)
    )
    own_rows = seq_rows // tp_size
    mixed = sent_and_summed(
        jnp.dot(attended, output_weight, preferred_element_type=jnp.float32).astype(jnp.bfloat16),
        "tp",
        0,
    )
    own_latent = lax.dynamic_slice_in_dim(latent[0], lax.axis_index("tp") * own_rows, own_rows, 0)
    updated = (own_latent.astype(jnp.float32) + vectors[2] * mixed).astype(jnp.bfloat16)
    whole = gathered_copies(updated, "tp", 0)
    return whole[None]


def solution(mesh):
    return jax.shard_map(
        on_device,
        mesh=mesh,
        in_specs=(
            P("dp", "sp", None),
            P("dp", "sp"),
            P("dp", "sp", None),
            P("sp"),
            P("sp", "tp"),
            P("sp", "tp"),
            P("sp", "tp"),
            P(),
            P(None, "tp"),
            P(None, "tp"),
            P(None, "tp"),
            P("tp", None),
            P(),
            P(),
            P("tp"),
        ),
        out_specs=P("dp", "sp", None),
        check_vma=False,
    )
```

profile of v0, /device:TPU:8, one launch (start us, length us, event | category | flops | bytes accessed | tf_op | source)
XLA Modules:
  0.0 259.9 jit_solution(298645395595733858)
XLA Ops:
  6.5 1.0 fusion.59
  11.3 1.1 broadcast_in_dim.12
  12.4 16.6 %all-to-all-start = ((f32[64,5,512]{2,1,0:T(8,128)}), f32[64,5,512]{2,1,0:T(8,128)S(1)}, u32[]{:S(2)}, u32[]{:S(2)}) async-start(f32[64,5,512]{2,1,0:T(8,128)} %broadcast_in_dim.12), calls=%async_computation | async-start | bytes 2097152 | tf_op jit(solution)/shard_map/all_to_all | solution.py:14
  29.0 2.1 fusion.16
  31.2 27.1 %all-to-all-done = f32[64,5,512]{2,1,0:T(8,128)S(1)} async-done(((f32[64,5,512]{2,1,0:T(8,128)}), f32[64,5,512]{2,1,0:T(8,128)S(1)}, u32[]{:S(2)}, u32[]{:S(2)}) %all-to-all-start) | async-done | bytes 655392 | tf_op jit(solution)/shard_map/all_to_all | solution.py:14
  59.0 4.3 %all-to-all-start.1 = ((f32[4,5,512]{2,1,0:T(8,128)}), f32[4,5,512]{2,1,0:T(8,128)S(1)}, u32[]{:S(2)}, u32[]{:S(2)}) async-start(f32[4,5,512]{2,1,0:T(8,128)} %broadcast_in_dim.13), calls=%async_computation.1 | async-start | bytes 131072 | tf_op jit(solution)/shard_map/all_to_all | solution.py:14
  63.3 1.3 add_rsqrt_fusion.2
  64.6 4.3 %all-to-all-done.1 = f32[4,5,512]{2,1,0:T(8,128)S(1)} async-done(((f32[4,5,512]{2,1,0:T(8,128)}), f32[4,5,512]{2,1,0:T(8,128)S(1)}, u32[]{:S(2)}, u32[]{:S(2)}) %all-to-all-start.1) | async-done | bytes 40992 | tf_op jit(solution)/shard_map/all_to_all | solution.py:14
  69.5 1.6 convolution_convert_fusion.1
  71.2 1.3 multiply_reduce_fusion.2
  74.8 1.4 copy.33
  76.5 1.1 multiply_reduce_fusion.3
  78.3 1.2 convolution_convert_fusion.2
  80.3 7.0 %all-to-all-start.2 = ((bf16[64,16,128]{2,1,0:T(8,128)(2,1)}), bf16[64,16,128]{2,1,0:T(8,128)(2,1)S(1)}, u32[]{:S(2)}, u32[]{:S(2)}) async-start(bf16[64,16,128]{2,1,0:T(8,128)(2,1)} %broadcast_in_dim.14), calls=%async_computation.2 | async-start | bytes 524288 | tf_op jit(solution)/shard_map/all_to_all | solution.py:14
  87.3 2.0 multiply_reduce_fusion.1
  89.7 10.9 %all-to-all-done.2 = bf16[64,16,128]{2,1,0:T(8,128)(2,1)S(1)} async-done(((bf16[64,16,128]{2,1,0:T(8,128)(2,1)}), bf16[64,16,128]{2,1,0:T(8,128)(2,1)S(1)}, u32[]{:S(2)}, u32[]{:S(2)}) %all-to-all-start.2) | async-done | bytes 262176 | tf_op jit(solution)/shard_map/all_to_all | solution.py:14
  102.1 1.0 fusion.25
  103.1 57.5 %all-gather.2.cloned.1.call-done = bf16[16384,128]{0,1:T(8,128)(2,1)} async-done(((bf16[256,128]{0,1:T(8,128)(2,1)}), bf16[16384,128]{0,1:T(8,128)(2,1)}) %all-gather.2.cloned.1.call-update) | async-done | bytes 4194320 | tf_op jit(solution)/shard_map/all_gather | solution.py:164
  160.6 6.4 %copy.38 = bf16[16384,128]{1,0:T(8,128)(2,1)} copy(bf16[16384,128]{0,1:T(8,128)(2,1)} %all-gather.2.cloned.1.call-done) | data formatting | bytes 8388608 | tf_op jit(solution)/shard_map/while | solution.py:185
  167.0 54.7 %while.14 = (s32[]{:T(128)}, f32[1024]{0:T(1024)S(1)}, f32[1024]{0:T(1024)S(1)}, f32[1024,64]{0,1:T(8,128)S(1)}, bf16[16,1024,128]{2,1,0:T(8,128)(2,1)}, /*index=5*/bf16[1024,64]{1,0:T(8,128)(2,1)S(1)}, s32[]{:T(128)}) while((s32[]{:T(128)}, f32[1024]{0:T(1024)S(1)}, f32[1024]{0:T(1024)S(1)}, f32[1024,64]{0,1:T(8,128)S(1)}, ...), condition=%wide.region_11.12_spmd, body=%wide.region_8.11_spmd.sunk | while | flops 276957184 | bytes 14352473 | solution.py:185
  170.4 1.0 dynamic-slice_bitcast_fusion.2
  173.8 1.0 dynamic-slice_bitcast_fusion.2
  177.2 1.0 dynamic-slice_bitcast_fusion.2
  184.1 1.0 dynamic-slice_bitcast_fusion.2
  187.5 1.0 dynamic-slice_bitcast_fusion.2
  190.9 1.0 dynamic-slice_bitcast_fusion.2
  194.3 1.0 dynamic-slice_bitcast_fusion.2
  197.8 1.0 dynamic-slice_bitcast_fusion.2
  221.9 1.4 convolution_convert_fusion
  223.3 4.2 %all-to-all-start.3 = ((bf16[4,64,2048]{2,1,0:T(8,128)(2,1)}), bf16[4,64,2048]{2,1,0:T(8,128)(2,1)S(1)}, u32[]{:S(2)}, u32[]{:S(2)}) async-start(bf16[4,64,2048]{2,1,0:T(8,128)(2,1)} %bitcast.36), calls=%async_computation.3 | async-start | bytes 2097152 | tf_op jit(solution)/shard_map/all_to_all | solution.py:41
  227.5 10.9 %all-to-all-done.3 = bf16[4,64,2048]{2,1,0:T(8,128)(2,1)S(1)} async-done(((bf16[4,64,2048]{2,1,0:T(8,128)(2,1)}), bf16[4,64,2048]{2,1,0:T(8,128)(2,1)S(1)}, u32[]{:S(2)}, u32[]{:S(2)}) %all-to-all-start.3) | async-done | bytes 1048608 | tf_op jit(solution)/shard_map/all_to_all | solution.py:41
  238.8 13.3 %all_to_all.25 = bf16[4,64,2048]{2,1,0:T(8,128)(2,1)S(1)} all-to-all(bf16[4,64,2048]{2,1,0:T(8,128)(2,1)S(1)} %broadcast_in_dim.17), channel_id=1, replica_groups=mesh['sp'=64,'tp'=4,'dp'=2] {'tp'}, dimensions={0} | all-to-all | bytes 2097152 | tf_op jit(solution)/shard_map/all_to_all | solution.py:14
  (163 shorter events, 58.7 us)
Async XLA Ops:
  6.5 215.3 %copy-start = (bf16[256,2048]{1,0:T(8,128)(2,1)S(1)}, bf16[256,2048]{1,0:T(8,128)(2,1)}, u32[]{:S(2)}) copy-start(bf16[256,2048]{1,0:T(8,128)(2,1)} %param.28) | copy-start | bytes 3145732
  6.5 63.0 %copy-start.1 = (bf16[1,256,2048]{2,1,0:T(8,128)(2,1)S(1)}, bf16[1,256,2048]{2,1,0:T(8,128)(2,1)}, u32[]{:S(2)}) copy-start(bf16[1,256,2048]{2,1,0:T(8,128)(2,1)} %param.17) | copy-start | bytes 3145732
  11.2 59.9 %copy-start.4 = (bf16[2048,64]{0,1:T(8,128)(2,1)S(1)}, bf16[2048,64]{0,1:T(8,128)(2,1)}, u32[]{:S(2)}) copy-start(bf16[2048,64]{0,1:T(8,128)(2,1)} %param.26) | copy-start | bytes 786436
  12.4 45.9 %all-to-all-start = ((f32[64,5,512]{2,1,0:T(8,128)}), f32[64,5,512]{2,1,0:T(8,128)S(1)}, u32[]{:S(2)}, u32[]{:S(2)}) async-start(f32[64,5,512]{2,1,0:T(8,128)} %broadcast_in_dim.12), calls=%async_computation | async-start | bytes 2097152 | tf_op jit(solution)/shard_map/all_to_all | solution.py:14
  58.3 16.5 %copy-start.2 = (bf16[2048,256]{1,0:T(8,128)(2,1)S(1)}, bf16[2048,256]{1,0:T(8,128)(2,1)}, u32[]{:S(2)}) copy-start(bf16[2048,256]{1,0:T(8,128)(2,1)} %param.25) | copy-start | bytes 3145732
  59.0 9.9 %all-to-all-start.1 = ((f32[4,5,512]{2,1,0:T(8,128)}), f32[4,5,512]{2,1,0:T(8,128)S(1)}, u32[]{:S(2)}, u32[]{:S(2)}) async-start(f32[4,5,512]{2,1,0:T(8,128)} %broadcast_in_dim.13), calls=%async_computation.1 | async-start | bytes 131072 | tf_op jit(solution)/shard_map/all_to_all | solution.py:14
  63.3 97.3 %all-gather.2.cloned.1.call-start = ((), (), s32[]{:S(2)}) async-start(), calls=%async_computation.5 | async-start | bytes 4259840 | tf_op jit(solution)/shard_map/all_gather | solution.py:164
  69.5 3.9 %copy-start.6 = (f32[1,4,512]{2,0,1:T(1,128)}, f32[1,4,512]{2,0,1:T(1,128)S(1)}, u32[]{:S(2)}) copy-start(f32[1,4,512]{2,0,1:T(1,128)S(1)} %get-tuple-element.93) | copy-start | bytes 24580
  69.5 3.9 %copy-start.7 = (f32[1,4,512]{2,0,1:T(1,128)}, f32[1,4,512]{2,0,1:T(1,128)S(1)}, u32[]{:S(2)}) copy-start(f32[1,4,512]{2,0,1:T(1,128)S(1)} %get-tuple-element.94) | copy-start | bytes 24580
  69.5 6.8 %copy-start.3 = (bf16[1,16,2048]{2,1,0:T(8,128)(2,1)S(1)}, bf16[1,16,2048]{2,1,0:T(8,128)(2,1)}, u32[]{:S(2)}) copy-start(bf16[1,16,2048]{2,1,0:T(8,128)(2,1)} %param.19) | copy-start | bytes 196612
  74.8 14.5 %copy-start.8 = (f32[64]{0:T(128)S(1)}, f32[64]{0:T(128)}, u32[]{:S(2)}) copy-start(f32[64]{0:T(128)} %param.29) | copy-start | bytes 772
  80.3 20.2 %all-to-all-start.2 = ((bf16[64,16,128]{2,1,0:T(8,128)(2,1)}), bf16[64,16,128]{2,1,0:T(8,128)(2,1)S(1)}, u32[]{:S(2)}, u32[]{:S(2)}) async-start(bf16[64,16,128]{2,1,0:T(8,128)(2,1)} %broadcast_in_dim.14), calls=%async_computation.2 | async-start | bytes 524288 | tf_op jit(solution)/shard_map/all_to_all | solution.py:14
  221.7 16.9 %copy-start.5 = (f32[1,4,512]{2,0,1:T(1,128)S(1)}, f32[1,4,512]{2,0,1:T(1,128)}, u32[]{:S(2)}) copy-start(f32[1,4,512]{2,0,1:T(1,128)} %get-tuple-element.90) | copy-start | bytes 24580
  223.3 15.1 %all-to-all-start.3 = ((bf16[4,64,2048]{2,1,0:T(8,128)(2,1)}), bf16[4,64,2048]{2,1,0:T(8,128)(2,1)S(1)}, u32[]{:S(2)}, u32[]{:S(2)}) async-start(bf16[4,64,2048]{2,1,0:T(8,128)(2,1)} %bitcast.36), calls=%async_computation.3 | async-start | bytes 2097152 | tf_op jit(solution)/shard_map/all_to_all | solution.py:41
Sparse Core Ops, SparseCore 0:
  74.2 86.3 all-gather.1
where the time goes:
time: 261 us; the launch traced here: 260 us
  waiting for transfers between devices  111 us (43%)
  matrix products  41.4 us (16%)
  starting transfers between devices  32.1 us (12%)
  local copies, waits for them, and re-layouts  28 us (11%)
  other arithmetic  20 us (8%)
  between operations  13.7 us (5%)
  blocking collectives  13.3 us (5%)
    all_gather x1, waiting for transfers between devices, on_device(): arrived = lax.all_gather(key_value, 'sp', axis=0, tiled=True)  57.5 us
    all_to_all x3, waiting for transfers between devices, from_everyone(): lax.all_to_all(jnp.broadcast_to(array[None], (size, *array.shape)), axis,...  42.3 us
    all_to_all x3, starting transfers between devices, from_everyone(): lax.all_to_all(jnp.broadcast_to(array[None], (size, *array.shape)), axis,...  27.8 us
    squeeze x16, local copies, waits for them, and re-layouts, on_device(): final_state, unused = lax.scan(absorb_block, start_state, blocks)  15.5 us
    dot_general x16, matrix products, absorb_block(): jnp.dot(weights.astype(jnp.bfloat16), pair_block[:, head_dim:], preferred...  14.9 us
    all_to_all x1, blocking collectives, from_everyone(): lax.all_to_all(jnp.broadcast_to(array[None], (size, *array.shape)), axis,...  13.3 us
    reduce_sum x16, other arithmetic, absorb_block(): weights.sum(axis=1)  11.7 us
    dot_general x16, matrix products, absorb_block(): jnp.dot(query_rows, pair_block[:, :head_dim].T, preferred_element_type=jn...  11.5 us
  transfers between devices with their start and end apart: 5, of which 5 were waited for; matrix products, arithmetic and copies ran while one was open for 6% of the time, Pallas kernels for 0%

commit v1 on v0

--- a/solution.py
+++ b/solution.py
@@ -161,7 +161,15 @@
             preferred_element_type=jnp.float32,
         ),
     )
-    arrived = lax.all_gather(key_value, "sp", axis=0, tiled=True)
+    arrived = jnp.concatenate(
+        lax.all_to_all(
+            jnp.stack(tuple((key_value for _ in range(lax.psum(1, axis_name="sp"))))),
+            axis_name="sp",
+            concat_axis=0,
+            split_axis=0,
+        ),
+        axis=0,
+    )
     arrived_rows = arrived.shape[0]
     block_rows = math.gcd(arrived_rows, 1024)
     blocks = arrived.reshape(arrived_rows // block_rows, block_rows, 2 * head_dim)

time: 261 us -> 306 us (1.17)
  the two profiles are of different devices: /device:TPU:8 before, /device:TPU:112 now
where the time goes in v1:
time: 306 us; the launch traced here: 305 us
  waiting for transfers between devices  167 us (55%)
  matrix products  40.4 us (13%)
  starting transfers between devices  39.4 us (13%)
  local copies, waits for them, and re-layouts  24.1 us (8%)
  other arithmetic  18.8 us (6%)
  blocking collectives  13.3 us (4%)
    all_to_all x1, waiting for transfers between devices, on_device(): lax.all_to_all(jnp.stack(tuple((key_value for _ in range(lax.psum(1, axis...  114 us
    all_to_all x3, waiting for transfers between devices, from_everyone(): lax.all_to_all(jnp.broadcast_to(array[None], (size, *array.shape)), axis,...  39.3 us
    all_to_all x3, starting transfers between devices, from_everyone(): lax.all_to_all(jnp.broadcast_to(array[None], (size, *array.shape)), axis,...  27.1 us
    squeeze x16, local copies, waits for them, and re-layouts, on_device(): final_state, unused = lax.scan(absorb_block, start_state, blocks)  15.5 us
    dot_general x16, matrix products, absorb_block(): jnp.dot(weights.astype(jnp.bfloat16), pair_block[:, head_dim:], preferred...  14.9 us
    all_to_all x1, waiting for transfers between devices, sent_and_summed(): pieces = lax.all_to_all(cut_along(array, dim, size), axis, 0, 0, tiled=True)  13.5 us
    all_to_all x1, blocking collectives, from_everyone(): lax.all_to_all(jnp.broadcast_to(array[None], (size, *array.shape)), axis,...  13.3 us
    reduce_sum x16, other arithmetic, absorb_block(): weights.sum(axis=1)  11.7 us
  transfers between devices with their start and end apart: 5, of which 5 were waited for; matrix products, arithmetic and copies ran while one was open for 4% of the time, Pallas kernels for 0%

profile of v1, /device:TPU:112, one launch (start us, length us, event | category | flops | bytes accessed | tf_op | source)
XLA Modules:
  0.0 304.5 jit_solution(18385532755915616692)
XLA Ops:
  0.0 1.1 fusion.59
  4.7 1.1 broadcast_in_dim.12
  5.8 15.1 %all-to-all-start = ((f32[64,5,512]{2,1,0:T(8,128)}), f32[64,5,512]{2,1,0:T(8,128)S(1)}, u32[]{:S(2)}, u32[]{:S(2)}) async-start(f32[64,5,512]{2,1,0:T(8,128)} %broadcast_in_dim.12), calls=%async_computation | async-start | bytes 2097152 | tf_op jit(solution)/shard_map/all_to_all | solution.py:14
  21.0 1.5 fusion.40
  22.6 1.5 fusion.16
  24.7 24.9 %all-to-all-done = f32[64,5,512]{2,1,0:T(8,128)S(1)} async-done(((f32[64,5,512]{2,1,0:T(8,128)}), f32[64,5,512]{2,1,0:T(8,128)S(1)}, u32[]{:S(2)}, u32[]{:S(2)}) %all-to-all-start) | async-done | bytes 655392 | tf_op jit(solution)/shard_map/all_to_all | solution.py:14
  50.3 4.3 %all-to-all-start.1 = ((f32[4,5,512]{2,1,0:T(8,128)}), f32[4,5,512]{2,1,0:T(8,128)S(1)}, u32[]{:S(2)}, u32[]{:S(2)}) async-start(f32[4,5,512]{2,1,0:T(8,128)} %broadcast_in_dim.13), calls=%async_computation.1 | async-start | bytes 131072 | tf_op jit(solution)/shard_map/all_to_all | solution.py:14
  55.3 5.0 %all-to-all-done.1 = f32[4,5,512]{2,1,0:T(8,128)S(1)} async-done(((f32[4,5,512]{2,1,0:T(8,128)}), f32[4,5,512]{2,1,0:T(8,128)S(1)}, u32[]{:S(2)}, u32[]{:S(2)}) %all-to-all-start.1) | async-done | bytes 40992 | tf_op jit(solution)/shard_map/all_to_all | solution.py:14
  60.3 1.2 convolution_convert_fusion.2
  61.5 1.1 multiply_reduce_fusion.3
  62.6 1.3 multiply_reduce_fusion.2
  65.5 7.7 %all-to-all-start.2 = ((bf16[64,16,128]{2,1,0:T(8,128)(2,1)}), bf16[64,16,128]{2,1,0:T(8,128)(2,1)S(1)}, u32[]{:S(2)}, u32[]{:S(2)}) async-start(bf16[64,16,128]{2,1,0:T(8,128)(2,1)} %broadcast_in_dim.14), calls=%async_computation.2 | async-start | bytes 524288 | tf_op jit(solution)/shard_map/all_to_all | solution.py:14
  74.2 9.5 %all-to-all-done.2 = bf16[64,16,128]{2,1,0:T(8,128)(2,1)S(1)} async-done(((bf16[64,16,128]{2,1,0:T(8,128)(2,1)}), bf16[64,16,128]{2,1,0:T(8,128)(2,1)S(1)}, u32[]{:S(2)}, u32[]{:S(2)}) %all-to-all-start.2) | async-done | bytes 262176 | tf_op jit(solution)/shard_map/all_to_all | solution.py:14
  83.6 3.0 stack.20
  86.6 8.8 %all-to-all-start.3 = ((bf16[64,256,128]{2,1,0:T(8,128)(2,1)}), bf16[64,256,128]{2,1,0:T(8,128)(2,1)}, u32[]{:S(2)}, u32[]{:S(2)}) async-start(bf16[64,256,128]{2,1,0:T(8,128)(2,1)} %stack.20), calls=%async_computation.3 | async-start | bytes 8388608 | tf_op jit(solution)/shard_map/all_to_all | solution.py:165
  95.6 1.4 copy.33
  97.1 1.9 multiply_reduce_fusion.1
  101.0 1.0 fusion.25
  102.0 114.5 %all-to-all-done.3 = bf16[64,256,128]{2,1,0:T(8,128)(2,1)} async-done(((bf16[64,256,128]{2,1,0:T(8,128)(2,1)}), bf16[64,256,128]{2,1,0:T(8,128)(2,1)}, u32[]{:S(2)}, u32[]{:S(2)}) %all-to-all-start.3) | async-done | bytes 4194336 | tf_op jit(solution)/shard_map/all_to_all | solution.py:165
  216.5 54.7 %while.14 = (s32[]{:T(128)}, f32[1024]{0:T(1024)S(1)}, f32[1024]{0:T(1024)S(1)}, f32[1024,64]{0,1:T(8,128)S(1)}, bf16[16,1024,128]{2,1,0:T(8,128)(2,1)}, /*index=5*/bf16[1024,64]{1,0:T(8,128)(2,1)S(1)}, s32[]{:T(128)}) while((s32[]{:T(128)}, f32[1024]{0:T(1024)S(1)}, f32[1024]{0:T(1024)S(1)}, f32[1024,64]{0,1:T(8,128)S(1)}, ...), condition=%wide.region_11.12_spmd, body=%wide.region_8.11_spmd.sunk | while | flops 276957184 | bytes 14352473 | solution.py:193
  219.9 1.0 dynamic-slice_bitcast_fusion.2
  223.4 1.0 dynamic-slice_bitcast_fusion.2
  226.8 1.0 dynamic-slice_bitcast_fusion.2
  230.2 1.0 dynamic-slice_bitcast_fusion.2
  233.6 1.0 dynamic-slice_bitcast_fusion.2
  237.0 1.0 dynamic-slice_bitcast_fusion.2
  240.4 1.0 dynamic-slice_bitcast_fusion.2
  243.9 1.0 dynamic-slice_bitcast_fusion.2
  271.4 1.4 convolution_convert_fusion
  272.8 3.5 %all-to-all-start.4 = ((bf16[4,64,2048]{2,1,0:T(8,128)(2,1)}), bf16[4,64,2048]{2,1,0:T(8,128)(2,1)S(1)}, u32[]{:S(2)}, u32[]{:S(2)}) async-start(bf16[4,64,2048]{2,1,0:T(8,128)(2,1)} %bitcast.36), calls=%async_computation.4 | async-start | bytes 2097152 | tf_op jit(solution)/shard_map/all_to_all | solution.py:41
  276.3 13.5 %all-to-all-done.4 = bf16[4,64,2048]{2,1,0:T(8,128)(2,1)S(1)} async-done(((bf16[4,64,2048]{2,1,0:T(8,128)(2,1)}), bf16[4,64,2048]{2,1,0:T(8,128)(2,1)S(1)}, u32[]{:S(2)}, u32[]{:S(2)}) %all-to-all-start.4) | async-done | bytes 1048608 | tf_op jit(solution)/shard_map/all_to_all | solution.py:41
  290.2 13.3 %all_to_all.30 = bf16[4,64,2048]{2,1,0:T(8,128)(2,1)S(1)} all-to-all(bf16[4,64,2048]{2,1,0:T(8,128)(2,1)S(1)} %broadcast_in_dim.17), channel_id=1, replica_groups=mesh['sp'=64,'tp'=4,'dp'=2] {'tp'}, dimensions={0} | all-to-all | bytes 2097152 | tf_op jit(solution)/shard_map/all_to_all | solution.py:14
  (169 shorter events, 57.9 us)
Async XLA Ops:
  0.0 271.4 %copy-start = (bf16[256,2048]{1,0:T(8,128)(2,1)S(1)}, bf16[256,2048]{1,0:T(8,128)(2,1)}, u32[]{:S(2)}) copy-start(bf16[256,2048]{1,0:T(8,128)(2,1)} %param.28) | copy-start | bytes 3145732
  0.0 60.3 %copy-start.3 = (bf16[1,16,2048]{2,1,0:T(8,128)(2,1)S(1)}, bf16[1,16,2048]{2,1,0:T(8,128)(2,1)}, u32[]{:S(2)}) copy-start(bf16[1,16,2048]{2,1,0:T(8,128)(2,1)} %param.19) | copy-start | bytes 196612
  0.0 62.6 %copy-start.1 = (bf16[1,256,2048]{2,1,0:T(8,128)(2,1)S(1)}, bf16[1,256,2048]{2,1,0:T(8,128)(2,1)}, u32[]{:S(2)}) copy-start(bf16[1,256,2048]{2,1,0:T(8,128)(2,1)} %param.17) | copy-start | bytes 3145732
  0.0 61.5 %copy-start.4 = (bf16[2048,64]{0,1:T(8,128)(2,1)S(1)}, bf16[2048,64]{0,1:T(8,128)(2,1)}, u32[]{:S(2)}) copy-start(bf16[2048,64]{0,1:T(8,128)(2,1)} %param.26) | copy-start | bytes 786436
  5.8 43.7 %all-to-all-start = ((f32[64,5,512]{2,1,0:T(8,128)}), f32[64,5,512]{2,1,0:T(8,128)S(1)}, u32[]{:S(2)}, u32[]{:S(2)}) async-start(f32[64,5,512]{2,1,0:T(8,128)} %broadcast_in_dim.12), calls=%async_computation | async-start | bytes 2097152 | tf_op jit(solution)/shard_map/all_to_all | solution.py:14
  49.7 23.5 %copy-start.7 = (f32[64]{0:T(128)S(1)}, f32[64]{0:T(128)}, u32[]{:S(2)}) copy-start(f32[64]{0:T(128)} %param.30) | copy-start | bytes 772
  49.7 23.7 %copy-start.5 = (bf16[2048,64]{0,1:T(8,128)(2,1)S(1)}, bf16[2048,64]{0,1:T(8,128)(2,1)}, u32[]{:S(2)}) copy-start(bf16[2048,64]{0,1:T(8,128)(2,1)} %param.27) | copy-start | bytes 786436
  49.7 23.7 %copy-start.6 = (f32[2048]{0:T(1024)S(1)}, f32[2048]{0:T(1024)}, u32[]{:S(2)}) copy-start(f32[2048]{0:T(1024)} %param.24) | copy-start | bytes 24580
  49.7 23.7 %copy-start.8 = (f32[256]{0:T(256)S(1)}, f32[256]{0:T(256)}, u32[]{:S(2)}) copy-start(f32[256]{0:T(256)} %add_rsqrt_fusion.2) | copy-start | bytes 3076
  50.3 9.9 %all-to-all-start.1 = ((f32[4,5,512]{2,1,0:T(8,128)}), f32[4,5,512]{2,1,0:T(8,128)S(1)}, u32[]{:S(2)}, u32[]{:S(2)}) async-start(f32[4,5,512]{2,1,0:T(8,128)} %broadcast_in_dim.13), calls=%async_computation.1 | async-start | bytes 131072 | tf_op jit(solution)/shard_map/all_to_all | solution.py:14
  65.5 18.1 %all-to-all-start.2 = ((bf16[64,16,128]{2,1,0:T(8,128)(2,1)}), bf16[64,16,128]{2,1,0:T(8,128)(2,1)S(1)}, u32[]{:S(2)}, u32[]{:S(2)}) async-start(bf16[64,16,128]{2,1,0:T(8,128)(2,1)} %broadcast_in_dim.14), calls=%async_computation.2 | async-start | bytes 524288 | tf_op jit(solution)/shard_map/all_to_all | solution.py:14
  86.6 8.9 %copy-start.11 = (f32[4]{0:T(128)S(1)}, f32[4]{0:T(128)}, u32[]{:S(2)}) copy-start(f32[4]{0:T(128)} %param.31) | copy-start | bytes 52
  86.6 9.0 %copy-start.2 = (bf16[2048,256]{1,0:T(8,128)(2,1)S(1)}, bf16[2048,256]{1,0:T(8,128)(2,1)}, u32[]{:S(2)}) copy-start(bf16[2048,256]{1,0:T(8,128)(2,1)} %param.25) | copy-start | bytes 3145732
  86.6 10.5 %copy-start.9 = (f32[256]{0:T(256)S(1)}, f32[256]{0:T(256)}, u32[]{:S(2)}) copy-start(f32[256]{0:T(256)} %add_rsqrt_fusion.2) | copy-start | bytes 3076
  86.6 129.9 %all-to-all-start.3 = ((bf16[64,256,128]{2,1,0:T(8,128)(2,1)}), bf16[64,256,128]{2,1,0:T(8,128)(2,1)}, u32[]{:S(2)}, u32[]{:S(2)}) async-start(bf16[64,256,128]{2,1,0:T(8,128)(2,1)} %stack.20), calls=%async_computation.3 | async-start | bytes 8388608 | tf_op jit(solution)/shard_map/all_to_all | solution.py:165
  95.5 3.6 %copy-start.10 = (f32[64]{0:T(128)S(1)}, f32[64]{0:T(128)}, u32[]{:S(2)}) copy-start(f32[64]{0:T(128)} %param.29) | copy-start | bytes 772
  272.8 17.1 %all-to-all-start.4 = ((bf16[4,64,2048]{2,1,0:T(8,128)(2,1)}), bf16[4,64,2048]{2,1,0:T(8,128)(2,1)S(1)}, u32[]{:S(2)}, u32[]{:S(2)}) async-start(bf16[4,64,2048]{2,1,0:T(8,128)(2,1)} %bitcast.36), calls=%async_computation.4 | async-start | bytes 2097152 | tf_op jit(solution)/shard_map/all_to_all | solution.py:41
